TPU v7x, 256 devices: a whole 4x4x8 slice. The times are simulated.
256 devices in a mesh: sp: 32 (over z, x), tp: 4 (over y), dp: 2 (over core).
Axes of the slice: x: 4, y: 4, z: 8, core: 2. Of those that a mesh axis runs over, the one named last changes fastest.
Arguments:
- latent: bfloat16 [2, 16384, 2048], P('dp', ('sp', 'tp')), may hold values from -6 to 6
- condition: float32 [2, 2048], P('dp'), may hold values from -6 to 6
- context: bfloat16 [2, 1024, 2048], P('dp', 'sp'), may hold values from -6 to 6
- context_cond: float32 [2048], replicated, may hold values from -6 to 6
- shift_matrix: bfloat16 [2048, 2048], P(('sp', 'tp')), may hold values from -0.125 to 0.125
- scale_matrix: bfloat16 [2048, 2048], P(('sp', 'tp')), may hold values from -0.125 to 0.125
- gate_matrix: bfloat16 [2048, 2048], P(('sp', 'tp')), may hold values from -0.125 to 0.125
- value_proj: bfloat16 [2048, 2048], P(None, 'tp'), may hold values from -0.125 to 0.125
- gate_proj: bfloat16 [2048, 2048], P(None, 'tp'), may hold values from -0.125 to 0.125
- write_proj: bfloat16 [2048, 1024], P(None, 'tp'), may hold values from -0.125 to 0.125
- read_proj: bfloat16 [2048, 1024], P(None, 'tp'), may hold values from -0.125 to 0.125
- step_proj: bfloat16 [2048, 2, 32], replicated, may hold values from -0.125 to 0.125
- decay_rate: float32 [2, 32], replicated, may hold values from 3.0456543e-05 to 0.0601
- pacing: float32 [2, 16384], P('dp'), may hold values from 0.2 to 4.3
- value_taps: float32 [5, 2048], replicated, may hold values from -2.5 to 2.5
- write_taps: float32 [5, 1024], replicated, may hold values from -2.5 to 2.5
- read_taps: float32 [5, 1024], replicated, may hold values from -2.5 to 2.5
- norm_gain: float32 [2048], replicated, may hold values from 0.1 to 1.9
- out_proj: bfloat16 [2048, 2048], P('tp'), may hold values from -0.125 to 0.125
Outputs:
- updated: bfloat16 [2, 16384, 2048], P('dp', ('sp', 'tp'))
All inputs are finite; a program needn't handle non-finite values.
Results may differ from a plain program's by a relative error of at most 0.006.
Values may be sent and summed in bfloat16 or wider, within the bound.
A program may use at most 128 MiB of HBM per device.

v0:
```python
import jax
import jax.numpy as jnp
from jax import lax
from jax.sharding import Mesh
from jax.sharding import PartitionSpec as P

HEAD = 64
STATE = 128
ROW = 64
BLOCK = 128
SP = ("sp_0", "sp_1")
SP_TP = ("sp_0", "sp_1", "tp")
NORM_FLOOR = 1e-05
GATED_FLOOR = 1e-06


def over_axes(value, axes):
    for axis in axes:
        value = lax.psum(value, axis)
    return value


def sent_together(arrays, axis, dim, along):
    widths = [a.shape[along] for a in arrays]
    both = jnp.concatenate(arrays, axis=along)
    result = lax.all_gather(both, axis, axis=dim, tiled=True)
    return tuple(jnp.split(result, [sum(widths[:k]) for k in range(1, len(widths))], axis=along))


def cut_along(value, dim, length):
    dims = value.shape
    pieces = value.reshape(*dims[:dim], length, dims[dim] // length, *dims[dim + 1 :])
    return jnp.moveaxis(pieces, dim, 0)


def sum_at_owner(value, axis, dim):
    pieces = cut_along(value, dim, lax.axis_size(axis))
    arrived = lax.all_to_all(pieces, axis, split_axis=0, concat_axis=0, tiled=True)
    return arrived.astype(jnp.float32).sum(axis=0)


def masked_exp(exponent, allowed):
    return jnp.where(allowed, jnp.exp(jnp.where(allowed, exponent, 0.0)), 0.0)


def modulate(row_block, shift_row, scale_row):
    values = row_block.astype(jnp.float32)
    center = jnp.mean(values, -1, keepdims=True)
    spread = jnp.mean(jnp.square(values - center), -1, keepdims=True)
    normed = (values - center) * lax.rsqrt(spread + NORM_FLOOR)
    return (normed * (1.0 + shift_row * 0.0 + scale_row) + shift_row).astype(jnp.bfloat16)


def convolve(values, kernel, run_count):
    length, channels = values.shape
    tap_count = kernel.shape[0]
    margin = tap_count // 2
    stretch = length // run_count
    blocked = values.astype(jnp.float32).reshape(run_count, stretch, channels)
    padded = jnp.pad(blocked, ((0, 0), (margin, margin), (0, 0)))
    summed = jnp.zeros_like(blocked)
    for offset in range(tap_count):
        summed = summed + padded[:, offset : offset + stretch] * kernel[offset]
    return jax.nn.silu(summed).reshape(length, channels).astype(jnp.bfloat16)


def context_state(values, writes, weight, groups):
    length = values.shape[0]
    per_group = weight.shape[1] // groups
    scaled = (
        writes.reshape(length, groups, 1, STATE) * weight.reshape(length, groups, per_group, 1)
    ).astype(jnp.bfloat16)
    head_values = values.reshape(length, groups, per_group, HEAD)
    return jnp.einsum("lgrn,lgrp->grnp", scaled, head_values, preferred_element_type=jnp.float32)


def block_inputs(values, writes, decays, steps, groups):
    length = values.shape[0]
    per_group = decays.shape[1] // groups
    blocks = length // BLOCK
    head_values = values.reshape(blocks, BLOCK, groups, per_group, HEAD)
    write_rows = writes.reshape(blocks, BLOCK, groups, STATE)
    cumulative = jnp.cumsum(decays.reshape(blocks, BLOCK, groups, per_group), axis=1)
    step_rows = steps.reshape(blocks, BLOCK, groups, per_group)
    weight = jnp.exp(cumulative[:, -1:] - cumulative) * step_rows
    scaled = (write_rows[:, :, :, None, :] * weight[..., None]).astype(jnp.bfloat16)
    increment = jnp.einsum(
        "kqgrn,kqgrp->kgrnp", scaled, head_values, preferred_element_type=jnp.float32
    )

    def advance(carry_state, paired):
        block_decay, block_increment = paired
        return (jnp.exp(block_decay)[..., None, None] * carry_state + block_increment, carry_state)

    empty_state = jnp.zeros(increment.shape[1:], jnp.float32)
    final_state, before = lax.scan(advance, empty_state, (cumulative[:, -1], increment))
    return (cumulative, final_state, before)


def block_outputs(values, reads, affinity, cumulative, steps, before, start):
    blocks, block_rows, groups, per_group = cumulative.shape
    head_values = values.reshape(blocks, block_rows, groups, per_group, HEAD)
    read_rows = reads.reshape(blocks, block_rows, groups, STATE).astype(jnp.float32)
    step_rows = steps.reshape(blocks, block_rows, groups, per_group)
    lower_mask = jnp.tril(jnp.ones((block_rows, block_rows), bool))[:, :, None, None]
    exponent = cumulative[:, :, None] - cumulative[:, None, :]
    mixing = (affinity[..., None] * masked_exp(exponent, lower_mask) * step_rows[:, None]).astype(
        jnp.bfloat16
    )
    within = jnp.einsum(
        "ktsgr,ksgrp->ktgrp", mixing, head_values, preferred_element_type=jnp.float32
    )
    block_decay = cumulative[:, -1]
    earlier = jnp.cumsum(block_decay, axis=0) - block_decay
    entering = before + jnp.exp(earlier)[..., None, None] * start[None]
    carried = jnp.einsum("ktgn,kgrnp->ktgrp", read_rows, entering) * jnp.exp(cumulative)[..., None]
    return (within + carried).reshape(blocks * block_rows, groups * per_group * HEAD)


def per_device(
    latent,
    condition,
    context,
    context_cond,
    shift_matrix,
    scale_matrix,
    gate_matrix,
    value_proj,
    gate_proj,
    write_proj,
    read_proj,
    step_proj,
    decay_rate,
    pacing,
    value_taps,
    write_taps,
    read_taps,
    norm_gain,
    out_proj,
):
    sp_count = lax.axis_size(SP)
    sp_index = lax.axis_index(SP)
    tp_index = lax.axis_index("tp")
    model_width = latent.shape[2]
    width_dev = value_proj.shape[1]
    keys_dev = write_proj.shape[1]
    heads_dev = width_dev // HEAD
    groups_dev = keys_dev // STATE
    state_shape = (groups_dev, heads_dev // groups_dev, STATE, HEAD)
    row_share = shift_matrix.shape[0]
    activated = jax.nn.silu(jnp.stack([condition[0], context_cond])).astype(jnp.bfloat16)
    own_cols = lax.dynamic_slice_in_dim(
        activated, (sp_index * lax.axis_size("tp") + tp_index) * row_share, row_share, 1
    )
    shift_part = jnp.dot(own_cols, shift_matrix, preferred_element_type=jnp.float32)
    scale_part = jnp.dot(own_cols, scale_matrix, preferred_element_type=jnp.float32)
    gate_part = jnp.dot(own_cols[:1], gate_matrix, preferred_element_type=jnp.float32)
    shifts, scales, gate_row = (
        over_axes(shift_part, SP_TP),
        over_axes(scale_part, SP_TP),
        over_axes(gate_part, SP_TP),
    )
    step_cols = lax.dynamic_slice_in_dim(step_proj, tp_index * heads_dev, heads_dev, 2).reshape(
        model_width, 2 * heads_dev
    )
    own_rows = modulate(latent[0], shifts[0], scales[0])
    row_piece = lax.all_gather(own_rows, "tp", axis=0, tiled=True)
    projected = jnp.concatenate(
        [
            jnp.dot(row_piece, value_proj, preferred_element_type=jnp.float32),
            jnp.dot(row_piece, gate_proj, preferred_element_type=jnp.float32),
            jnp.dot(row_piece, write_proj, preferred_element_type=jnp.float32),
            jnp.dot(row_piece, read_proj, preferred_element_type=jnp.float32),
            jnp.dot(row_piece, step_cols, preferred_element_type=jnp.float32),
        ],
        axis=1,
    )
    tokens = projected.shape[0]
    run_count = tokens // ROW
    gate_end = 2 * width_dev
    write_end = gate_end + keys_dev
    read_end = write_end + keys_dev
    value_kernel = lax.dynamic_slice_in_dim(value_taps, tp_index * width_dev, width_dev, 1)
    write_kernel = lax.dynamic_slice_in_dim(write_taps, tp_index * keys_dev, keys_dev, 1)
    read_kernel = lax.dynamic_slice_in_dim(read_taps, tp_index * keys_dev, keys_dev, 1)
    values = convolve(projected[:, :width_dev].astype(jnp.bfloat16), value_kernel, run_count)
    gate_pre = projected[:, width_dev:gate_end].astype(jnp.bfloat16)
    writes = convolve(
        projected[:, gate_end:write_end].astype(jnp.bfloat16), write_kernel, run_count
    )
    reads = convolve(projected[:, write_end:read_end].astype(jnp.bfloat16), read_kernel, run_count)
    step_raw = projected[:, read_end:].astype(jnp.bfloat16)
    latent_raw = (
        lax.optimization_barrier(step_raw).astype(jnp.float32).reshape(tokens, 2, heads_dev)
    )
    rates = lax.dynamic_slice_in_dim(decay_rate, tp_index * heads_dev, heads_dev, 1)
    local_pace = lax.dynamic_slice_in_dim(pacing[0], sp_index * tokens, tokens, 0)
    forward_step = jax.nn.softplus(latent_raw[:, 0]) * local_pace[:, None]
    forward_decay = -rates[0][None, :] * forward_step
    backward_step = jax.nn.softplus(latent_raw[:, 1]) * local_pace[:, None]
    backward_decay = -rates[1][None, :] * backward_step
    forward_cumul, forward_end, forward_before = block_inputs(
        values, writes, forward_decay, forward_step, groups_dev
    )
    backward_cumul, backward_end, backward_before = block_inputs(
        values[::-1], writes[::-1], backward_decay[::-1], backward_step[::-1], groups_dev
    )
    context_hidden = modulate(context[0], shifts[1], scales[1])
    context_value = jnp.dot(context_hidden, value_proj, preferred_element_type=jnp.float32).astype(
        jnp.bfloat16
    )
    context_write = jnp.dot(context_hidden, write_proj, preferred_element_type=jnp.float32).astype(
        jnp.bfloat16
    )
    context_raw = jnp.dot(context_hidden, step_cols, preferred_element_type=jnp.float32).astype(
        jnp.bfloat16
    )
    ctx_value_all, ctx_write_all, ctx_raw_all, latent_raw_all = (
        *sent_together((context_value, context_write, context_raw), SP, 0, 1),
        lax.all_gather(step_raw, SP, axis=0, tiled=True),
    )
    ctx_values = convolve(ctx_value_all, value_kernel, 1)
    ctx_writes = convolve(ctx_write_all, write_kernel, 1)
    ctx_raw = lax.optimization_barrier(ctx_raw_all).astype(jnp.float32).reshape(-1, 2, heads_dev)
    ctx_fwd_step = jax.nn.softplus(ctx_raw[:, 0])
    ctx_fwd_decay = -rates[0][None, :] * ctx_fwd_step
    ctx_cumul = jnp.cumsum(ctx_fwd_decay, axis=0)
    ctx_forward = context_state(
        ctx_values, ctx_writes, jnp.exp(ctx_cumul[-1:] - ctx_cumul) * ctx_fwd_step, groups_dev
    )
    ctx_bwd_step = jax.nn.softplus(ctx_raw[:, 1])
    ctx_bwd_decay = -rates[1][None, :] * ctx_bwd_step
    ctx_back_cumul = jnp.cumsum(ctx_bwd_decay, axis=0)
    ctx_backward = context_state(
        ctx_values, ctx_writes, jnp.exp(ctx_back_cumul - ctx_bwd_decay) * ctx_bwd_step, groups_dev
    )
    ctx_forward = ctx_forward.reshape(heads_dev, STATE, HEAD)
    ctx_backward = ctx_backward.reshape(heads_dev, STATE, HEAD)
    empty_state = jnp.zeros((heads_dev, STATE, HEAD), jnp.float32)
    all_raw = (
        lax.optimization_barrier(latent_raw_all)
        .astype(jnp.float32)
        .reshape(sp_count, tokens, 2, heads_dev)
    )
    all_steps = jax.nn.softplus(all_raw) * pacing[0].reshape(sp_count, tokens)[:, :, None, None]
    totals = jnp.sum(-rates[None, None] * all_steps, axis=1)
    forward_totals = totals[:, 0]
    backward_totals = totals[:, 1]
    forward_prefix = jnp.cumsum(forward_totals, axis=0) - forward_totals
    backward_suffix = jnp.cumsum(backward_totals[::-1], axis=0)[::-1] - backward_totals
    forward_through = forward_prefix + forward_totals
    backward_through = backward_suffix + backward_totals
    own_prefix = forward_prefix[sp_index]
    own_suffix = backward_suffix[sp_index]
    forward_piece, backward_piece = tuple(
        (
            part.astype(jnp.float32)
            for part in sent_together(
                (
                    forward_end.reshape(1, heads_dev, STATE, HEAD).astype(jnp.bfloat16),
                    backward_end.reshape(1, heads_dev, STATE, HEAD).astype(jnp.bfloat16),
                ),
                SP,
                0,
                1,
            )
        )
    )
    shard_count = forward_piece.shape[0]
    sources = jnp.arange(shard_count)
    forward_gap = own_prefix[None] - forward_through
    backward_gap = own_suffix[None] - backward_through
    forward_weight = masked_exp(forward_gap, (sources < sp_index)[:, None])
    backward_weight = masked_exp(backward_gap, (sources > sp_index)[:, None])
    forward_in = empty_state + jnp.sum(forward_weight[:, :, None, None] * forward_piece, axis=0)
    backward_in = empty_state + jnp.sum(backward_weight[:, :, None, None] * backward_piece, axis=0)
    forward_start = forward_in + jnp.exp(own_prefix)[:, None, None] * ctx_forward
    backward_start = backward_in + jnp.exp(own_suffix)[:, None, None] * ctx_backward
    blocks = tokens // BLOCK
    forward_affinity = jnp.einsum(
        "ktgn,ksgn->ktsg",
        reads.reshape(blocks, BLOCK, groups_dev, STATE),
        writes.reshape(blocks, BLOCK, groups_dev, STATE),
        preferred_element_type=jnp.float32,
    )
    backward_affinity = forward_affinity[::-1, ::-1, ::-1]
    forward_out = block_outputs(
        values,
        reads,
        forward_affinity,
        forward_cumul,
        forward_step,
        forward_before,
        forward_start.reshape(state_shape),
    )
    backward_out = block_outputs(
        values[::-1],
        reads[::-1],
        backward_affinity,
        backward_cumul,
        backward_step[::-1],
        backward_before,
        backward_start.reshape(state_shape),
    )[::-1]
    gated_heads = (forward_out + backward_out) * jax.nn.silu(gate_pre.astype(jnp.float32))
    grouped = gated_heads.reshape(tokens, groups_dev, -1)
    grouped = grouped * lax.rsqrt(jnp.mean(grouped * grouped, -1, keepdims=True) + GATED_FLOOR)
    gain_dev = lax.dynamic_slice_in_dim(norm_gain, tp_index * width_dev, width_dev, 0)
    inner_rows = (grouped.reshape(tokens, width_dev) * gain_dev).astype(jnp.bfloat16)
    mixed = sum_at_owner(
        jnp.dot(inner_rows, out_proj, preferred_element_type=jnp.float32).astype(jnp.bfloat16),
        "tp",
        0,
    ).astype(jnp.bfloat16)
    updated = (
        latent[0].astype(jnp.float32)
        + gate_row[0] * lax.optimization_barrier(mixed).astype(jnp.float32)
    ).astype(jnp.bfloat16)
    return updated[None]


def solution(mesh):
    torus = Mesh(
        mesh.devices.reshape(8, 4, mesh.shape["tp"], mesh.shape["dp"]), ("sp_0", "sp_1", "tp", "dp")
    )
    placed = (
        P("dp", SP_TP, None),
        P("dp", None),
        P("dp", SP, None),
        P(),
        P(SP_TP, None),
        P(SP_TP, None),
        P(SP_TP, None),
        P(None, "tp"),
        P(None, "tp"),
        P(None, "tp"),
        P(None, "tp"),
        P(),
        P(),
        P("dp", None),
        P(),
        P(),
        P(),
        P(),
        P("tp", None),
    )
    return jax.shard_map(
        per_device, mesh=torus, in_specs=placed, out_specs=P("dp", SP_TP, None), check_vma=False
    )
```

profile of v0, /device:TPU:8, one launch (start us, length us, event | category | flops | bytes accessed | tf_op | source)
XLA Modules:
  0.0 367.3 jit_solution(16203024841715670939)
XLA Ops:
  13.0 33.2 %all-reduce.5 = (f32[2,2048]{1,0:T(2,128)S(1)}, f32[2,2048]{1,0:T(2,128)S(1)}, f32[1,2048]{1,0:T(1,128)S(1)}) all-reduce(f32[2,2048]{1,0:T(2,128)S(1)} %fusion.172, f32[2,2048]{1,0:T(2,128)S(1)} %fusion.173, f32[1,2048]{1,0:T(1,128)S(1)} %fusion.153), channel_id=1, replica_groups=mesh['sp_0'=8,'sp_1'=4,'tp'=4,'dp'=2] {'sp_0'}, use_global_device_ids=true, to_apply=%region_5.6 | all-reduce | flops 10240 | bytes 81920 | tf_op jit(solution)/shard_map/psum | solution.py:19
  46.1 17.4 %all-reduce.7 = (f32[2,2048]{1,0:T(2,128)S(1)}, f32[2,2048]{1,0:T(2,128)S(1)}, f32[1,2048]{1,0:T(1,128)S(1)}) all-reduce(f32[2,2048]{1,0:T(2,128)S(1)} %get-tuple-element.183, f32[2,2048]{1,0:T(2,128)S(1)} %get-tuple-element.184, f32[1,2048]{1,0:T(1,128)S(1)} %get-tuple-element.185), channel_id=1, replica_groups=mesh['sp_0'=8,'sp_1'=4,'tp'=4,'dp'=2] {'sp_1'}, use_global_device_ids=true, to_apply=%region_6.7 | all-reduce | flops 10240 | bytes 81920 | tf_op jit(solution)/shard_map/psum | solution.py:19
  63.5 15.2 %all-reduce.6 = (f32[2,2048]{1,0:T(2,128)S(1)}, f32[2,2048]{1,0:T(2,128)S(1)}, f32[2048]{0:T(1024)}) all-reduce(f32[2,2048]{1,0:T(2,128)S(1)} %get-tuple-element.189, f32[2,2048]{1,0:T(2,128)S(1)} %get-tuple-element.190, f32[2048]{0:T(1024)S(1)} %bitcast.366), channel_id=1, replica_groups=mesh['sp_0'=8,'sp_1'=4,'tp'=4,'dp'=2] {'tp'}, use_global_device_ids=true, to_apply=%region_7.8 | all-reduce | flops 10240 | bytes 81920 | tf_op jit(solution)/shard_map/psum | solution.py:19
  91.0 20.2 %all-gather.4.cloned.1.call-done = bf16[512,2048]{1,0:T(8,128)(2,1)} async-done(((bf16[128,2048]{1,0:T(8,128)(2,1)}), bf16[512,2048]{1,0:T(8,128)(2,1)}) %all-gather.4.cloned.1.call-update) | async-done | bytes 2097168 | tf_op jit(solution)/shard_map/all_gather | solution.py:167
  118.4 2.7 fusion.169
  122.3 3.5 convolution_convert_fusion.2
  127.6 8.3 %rev.32 = bf16[512,512]{1,0:T(8,128)(2,1)} reverse(bf16[512,512]{1,0:T(8,128)(2,1)} %bitcast.310), dimensions={0} | reverse | bytes 1048576 | tf_op jit(solution)/shard_map/rev | solution.py:206
  135.9 2.9 reshape.563
  144.2 2.6 rev.30
  150.0 3.6 fusion.75
  155.2 8.1 %while.27 = (s32[]{:T(128)}, f32[2,4,128,64]{3,2,1,0:T(8,128)S(1)}, f32[4,2,4,128,64]{4,3,2,1,0:T(8,128)}, f32[4,2,4]{2,1,0:T(2,128)S(1)}, f32[4,2,4,128,64]{4,3,2,1,0:T(8,128)}, /*index=5*/s32[]{:T(128)}, s32[]{:T(128)}) while((s32[]{:T(128)}, f32[2,4,128,64]{3,2,1,0:T(8,128)S(1)}, f32[4,2,4,128,64]{4,3,2,1,0:T(8,128)}, ...), condition=%wide.region_19.20_spmd.clone, body=%wide.region_18.19_spmd.clone.sunk | while | flops 262147 | bytes 1573568 | solution.py:96
  169.6 2.9 reshape.562
  182.2 10.8 %while.26 = (s32[]{:T(128)}, f32[2,4,128,64]{3,2,1,0:T(8,128)S(1)}, f32[4,2,4,128,64]{4,3,2,1,0:T(8,128)}, f32[4,2,4]{2,1,0:T(2,128)}, f32[4,2,4,128,64]{4,3,2,1,0:T(8,128)}, /*index=5*/s32[]{:T(128)}, s32[]{:T(128)}) while((s32[]{:T(128)}, f32[2,4,128,64]{3,2,1,0:T(8,128)S(1)}, f32[4,2,4,128,64]{4,3,2,1,0:T(8,128)}, ...), condition=%wide.region_13.14_spmd.clone, body=%wide.region_12.13_spmd.clone.sunk | while | flops 262147 | bytes 1573568 | solution.py:96
  211.6 2.8 fusion.118
  214.4 2.7 reshape.555
  220.4 3.8 %multiply_convert_fusion.5 = bf16[1,1024,512]{1,2,0:T(8,128)(2,1)} fusion(f32[1,1024,512]{1,2,0:T(8,128)S(1)} %convert_bitcast_fusion, bf16[1024,512]{0,1:T(8,128)(2,1)S(1)} %copy.289, f32[512]{0:T(512)S(1)} %bitcast.351, f32[512]{0:T(512)S(1)} %bitcast.345, f32[512]{0:T(512)S(1)} %bitcast.347, f32[512]{0:T(512)S(1)} %bitcast.349, f32[512]{0:T(512)S(1)} %bitcast.343), kind=kLoop, calls=%fused_computation.37 | loop fusion | flops 7864320 | bytes 4204544 | tf_op jit(solution)/shard_map/convert_element_type | solution.py:64
  230.3 3.0 rev.33
  234.1 51.8 %all_gather.13 = bf16[16384,16]{0,1:T(8,128)(2,1)S(1)} all-gather(bf16[512,16]{0,1:T(8,128)(2,1)S(1)} %convolution_convert_fusion.7), channel_id=1, replica_groups=mesh['sp_0'=8,'sp_1'=4,'tp'=4,'dp'=2] {'sp_0','sp_1'}, dimensions={0}, use_global_device_ids=true | all-gather | bytes 540672 | tf_op jit(solution)/shard_map/all_gather | solution.py:220
  295.7 2.9 rev.36
  303.1 2.9 convolution_bitcast_fusion.1
  308.0 4.5 %multiply_reduce_fusion.1 = (f32[8,128,64]{1,2,0:T(8,128)S(1)}, f32[8,128,64]{1,2,0:T(8,128)S(1)}) fusion(bf16[32,16,128,64]{2,3,1,0:T(8,128)(2,1)} %all-gather.6.cloned.1.call-done, f32[32,8]{1,0:T(8,128)S(1)} %exponential_select_fusion.1, f32[32,8]{1,0:T(8,128)S(1)} %get-tuple-element.211), kind=kLoop, calls=%fused_computation.7 | loop fusion | flops 12451840 | bytes 8914944 | tf_op jit(solution)/shard_map/reduce_sum | solution.py:275
  324.0 6.0 %rev.37 = f32[512,512]{0,1:T(8,128)} reverse(f32[512,512]{0,1:T(8,128)S(1)} %bitcast.312), dimensions={0} | reverse | bytes 2097152 | tf_op jit(solution)/shard_map/rev | solution.py:296
  329.9 4.3 %bitcast_reduce_fusion = (f32[512,2]{0,1:T(2,128)S(1)}, f32[512,512]{0,1:T(8,128)S(1)}) fusion(bf16[512,2048]{1,0:T(8,128)(2,1)} %all-gather.4.cloned.1.call-done, bf16[2048,512]{1,0:T(8,128)(2,1)} %param.31, f32[512,512]{0,1:T(8,128)} %rev.37, f32[64,8,4,128]{3,2,1,0:T(4,128)} %bitcast.318), kind=kOutput, calls=%fused_computation.119 | convolution fusion | flops 1076362240 | bytes 7344128 | tf_op jit(solution)/shard_map/dot_general | solution.py:171
  335.8 21.9 %all_to_all.5 = bf16[4,128,2048]{2,1,0:T(8,128)(2,1)} all-to-all(bf16[4,128,2048]{2,1,0:T(8,128)(2,1)S(1)} %bitcast.316), channel_id=1, replica_groups=mesh['sp_0'=8,'sp_1'=4,'tp'=4,'dp'=2] {'tp'}, dimensions={0} | all-to-all | bytes 4194304 | tf_op jit(solution)/shard_map/all_to_all | solution.py:38
  (308 shorter events, 133.6 us)
Async XLA Ops:
  6.5 328.0 %copy-start = (bf16[512,2048]{1,0:T(8,128)(2,1)S(1)}, bf16[512,2048]{1,0:T(8,128)(2,1)}, u32[]{:S(2)}) copy-start(bf16[512,2048]{1,0:T(8,128)(2,1)} %param.41) | copy-start | bytes 6291460
  6.5 74.5 %copy-start.14 = (bf16[1,32,2048]{2,1,0:T(8,128)(2,1)S(1)}, bf16[1,32,2048]{2,1,0:T(8,128)(2,1)}, u32[]{:S(2)}) copy-start(bf16[1,32,2048]{2,1,0:T(8,128)(2,1)} %param.25) | copy-start | bytes 393220
  6.5 76.0 %copy-start.16 = (bf16[2048,256]{1,0:T(8,128)(2,1)S(1)}, bf16[2048,256]{1,0:T(8,128)(2,1)}, u32[]{:S(2)}) copy-start(bf16[2048,256]{1,0:T(8,128)(2,1)} %param.32) | copy-start | bytes 3145732
  6.5 104.7 %all-gather.4.cloned.1.call-start = ((), (), s32[]{:S(2)}) async-start(), calls=%async_computation.1 | async-start | bytes 2621440 | tf_op jit(solution)/shard_map/all_gather | solution.py:167
  81.0 118.0 %all-gather.8.cloned.1.call-start = ((), (), s32[]{:S(2)}) async-start(), calls=%async_computation.3 | async-start | bytes 1892352 | tf_op jit(solution)/shard_map/all_gather | solution.py:26
  85.7 222.3 %all-gather.6.cloned.1.call-start = ((), (), s32[]{:S(2)}) async-start(), calls=%async_computation.2 | async-start | bytes 8650752 | tf_op jit(solution)/shard_map/all_gather | solution.py:26
  86.9 31.5 %copy-start.56 = (f32[8]{0:T(128)}, f32[8]{0:T(128)S(1)}, u32[]{:S(2)}) copy-start(f32[8]{0:T(128)S(1)} %get-tuple-element.232) | copy-start | bytes 100
  89.2 36.8 %copy-start.31 = (f32[1,512]{1,0:T(1,128)}, f32[1,512]{1,0:T(1,128)S(1)}, u32[]{:S(2)}) copy-start(f32[1,512]{1,0:T(1,128)S(1)} %get-tuple-element.204) | copy-start | bytes 6148
  89.2 36.8 %copy-start.33 = (f32[1,512]{1,0:T(1,128)}, f32[1,512]{1,0:T(1,128)S(1)}, u32[]{:S(2)}) copy-start(f32[1,512]{1,0:T(1,128)S(1)} %get-tuple-element.205) | copy-start | bytes 6148
  89.2 36.8 %copy-start.35 = (f32[1,512]{1,0:T(1,128)}, f32[1,512]{1,0:T(1,128)S(1)}, u32[]{:S(2)}) copy-start(f32[1,512]{1,0:T(1,128)S(1)} %get-tuple-element.206) | copy-start | bytes 6148
  89.2 36.8 %copy-start.37 = (f32[1,512]{1,0:T(1,128)}, f32[1,512]{1,0:T(1,128)S(1)}, u32[]{:S(2)}) copy-start(f32[1,512]{1,0:T(1,128)S(1)} %get-tuple-element.207) | copy-start | bytes 6148
  89.2 36.8 %copy-start.39 = (f32[1,512]{1,0:T(1,128)}, f32[1,512]{1,0:T(1,128)S(1)}, u32[]{:S(2)}) copy-start(f32[1,512]{1,0:T(1,128)S(1)} %get-tuple-element.208) | copy-start | bytes 6148
  90.9 52.8 %copy-start.45 = (f32[1,256]{1,0:T(1,128)}, f32[1,256]{1,0:T(1,128)S(1)}, u32[]{:S(2)}) copy-start(f32[1,256]{1,0:T(1,128)S(1)} %get-tuple-element.215) | copy-start | bytes 3076
  90.9 52.8 %copy-start.47 = (f32[1,256]{1,0:T(1,128)}, f32[1,256]{1,0:T(1,128)S(1)}, u32[]{:S(2)}) copy-start(f32[1,256]{1,0:T(1,128)S(1)} %get-tuple-element.216) | copy-start | bytes 3076
  91.0 52.8 %copy-start.49 = (f32[1,256]{1,0:T(1,128)}, f32[1,256]{1,0:T(1,128)S(1)}, u32[]{:S(2)}) copy-start(f32[1,256]{1,0:T(1,128)S(1)} %get-tuple-element.217) | copy-start | bytes 3076
  91.0 52.8 %copy-start.51 = (f32[1,256]{1,0:T(1,128)}, f32[1,256]{1,0:T(1,128)S(1)}, u32[]{:S(2)}) copy-start(f32[1,256]{1,0:T(1,128)S(1)} %get-tuple-element.218) | copy-start | bytes 3076
  91.0 52.8 %copy-start.53 = (f32[1,256]{1,0:T(1,128)}, f32[1,256]{1,0:T(1,128)S(1)}, u32[]{:S(2)}) copy-start(f32[1,256]{1,0:T(1,128)S(1)} %get-tuple-element.219) | copy-start | bytes 3076
  182.2 12.3 %copy-start.23 = (f32[1,16384]{1,0:T(1,128)S(1)}, f32[1,16384]{1,0:T(1,128)}, u32[]{:S(2)}) copy-start(f32[1,16384]{1,0:T(1,128)} %param.36) | copy-start | bytes 196612
  228.0 57.8 %copy-start.28 = (f32[32,512]{1,0:T(8,128)S(1)}, f32[32,512]{1,0:T(8,128)}, u32[]{:S(2)}) copy-start(f32[32,512]{1,0:T(8,128)} %mul.746) | copy-start | bytes 196612
  234.1 61.7 %copy-start.9 = (bf16[8,64,256]{2,1,0:T(8,128)(2,1)S(1)}, bf16[8,64,256]{2,1,0:T(8,128)(2,1)}, u32[]{:S(2)}) copy-start(bf16[8,64,256]{2,1,0:T(8,128)(2,1)} %copy-done.8) | copy-start | bytes 786436
  285.8 17.2 %copy-start.13 = (bf16[4,128,2,4,64]{1,4,3,2,0:T(8,128)(2,1)S(1)}, bf16[4,128,2,4,64]{1,4,3,2,0:T(8,128)(2,1)}, u32[]{:S(2)}) copy-start(bf16[4,128,2,4,64]{1,4,3,2,0:T(8,128)(2,1)} %copy-done.12) | copy-start | bytes 1572868
  285.9 17.2 %copy-start.26 = (f32[4,128,2,4]{1,3,2,0:T(4,128)S(1)}, f32[4,128,2,4]{1,3,2,0:T(4,128)}, u32[]{:S(2)}) copy-start(f32[4,128,2,4]{1,3,2,0:T(4,128)} %get-tuple-element.195) | copy-start | bytes 49156
  285.9 17.2 %copy-start.27 = (f32[4,128,2,4]{1,3,2,0:T(4,128)S(1)}, f32[4,128,2,4]{1,3,2,0:T(4,128)}, u32[]{:S(2)}) copy-start(f32[4,128,2,4]{1,3,2,0:T(4,128)} %copy.232) | copy-start | bytes 49156
  285.9 17.2 %copy-start.42 = (pred[128,128]{1,0:T(8,128)(4,1)S(1)}, pred[128,128]{1,0:T(8,128)(4,1)}, u32[]{:S(2)}) copy-start(pred[128,128]{1,0:T(8,128)(4,1)} %iota_compare_fusion) | copy-start | bytes 49156
  (50 other events, 167.0 us)
Sparse Core Ops, SparseCore 0:
  81.1 30.1 all-gather.3
  113.8 78.5 all-gather.7
  195.0 100.4 all-gather.5
where the time goes:
time: 371 us; the launch traced here: 367 us
  blocking collectives  139 us (37%)
  local copies, waits for them, and re-layouts  88 us (24%)
  other arithmetic  63.3 us (17%)
  matrix products  41.8 us (11%)
  waiting for transfers between devices  20.3 us (5%)
  between operations  14.3 us (4%)
    psum x3, blocking collectives, over_axes(): value = lax.psum(value, axis)  65.7 us
    all_gather x1, blocking collectives, per_device(): lax.all_gather(step_raw, SP, axis=0, tiled=True)  51.8 us
    all_to_all x1, blocking collectives, sum_at_owner(): lax.all_to_all(pieces, axis, split_axis=0, concat_axis=0, tiled=True)  21.9 us
    all_gather x1, waiting for transfers between devices, per_device(): row_piece = lax.all_gather(own_rows, 'tp', axis=0, tiled=True)  20.2 us
    add x8, other arithmetic, advance(): jnp.exp(block_decay)[..., None, None] * carry_state + block_increment  9.3 us
    rev x1, local copies, waits for them, and re-layouts, per_device(): values[::-1]  8.32 us
  transfers between devices with their start and end apart: 3, of which 1 were waited for; matrix products, arithmetic and copies ran while one was open for 41% of the time, Pallas kernels for 0%

commit v1 on v0

--- a/solution.py
+++ b/solution.py
@@ -16,7 +16,7 @@
 
 def over_axes(value, axes):
     for axis in axes:
-        value = lax.psum(value, axis)
+        value = jnp.sum(lax.all_gather(value, axis), axis=0)
     return value
 
 

time: 371 us -> 439 us (1.18)
  blocking collectives: 139 us -> 202 us
  starting transfers between devices: 0.09 us -> 6.09 us
    all_gather x0 -> x9, blocking collectives: none -> 150 us  [over_axes(): value = jnp.sum(lax.all_gather(value, axis), axis=0)]
    psum x3 -> x0, blocking collectives: 65.7 us -> none  [over_axes(): value = lax.psum(value, axis)]
    all_to_all x1 -> x0, blocking collectives: 21.9 us -> none  [sum_at_owner(): lax.all_to_all(pieces, axis, split_axis=0, concat_axis=0, tiled=True)]
    all_to_all x0 -> x1, starting transfers between devices: none -> 6 us  [sum_at_owner(): lax.all_to_all(pieces, axis, split_axis=0, concat_axis=0, tiled=True)]
  transfers between devices with their start and end apart: 3 -> 4, of which waited for: 1 -> 1; matrix products, arithmetic and copies ran while one was open for 41% -> 35% of each run, Pallas kernels for 0% -> 0%
where the time goes in v1:
time: 439 us; the launch traced here: 435 us
  blocking collectives  202 us (46%)
  local copies, waits for them, and re-layouts  84.3 us (19%)
  other arithmetic  64.1 us (15%)
  matrix products  44 us (10%)
  waiting for transfers between devices  20.8 us (5%)
  between operations  14.2 us (3%)
  starting transfers between devices  6.09 us (1%)
    all_gather x9, blocking collectives, over_axes(): value = jnp.sum(lax.all_gather(value, axis), axis=0)  150 us
    all_gather x1, blocking collectives, per_device(): lax.all_gather(step_raw, SP, axis=0, tiled=True)  52.2 us
    all_gather x1, waiting for transfers between devices, per_device(): row_piece = lax.all_gather(own_rows, 'tp', axis=0, tiled=True)  20.7 us
    add x8, other arithmetic, advance(): jnp.exp(block_decay)[..., None, None] * carry_state + block_increment  9.3 us
  transfers between devices with their start and end apart: 4, of which 1 were waited for; matrix products, arithmetic and copies ran while one was open for 35% of the time, Pallas kernels for 0%

profile of v1, /device:TPU:8, one launch (start us, length us, event | category | flops | bytes accessed | tf_op | source)
XLA Modules:
  0.0 435.4 jit_solution(7170426092652810444)
XLA Ops:
  8.4 28.3 %all-gather.12 = f32[8,2,2048]{2,1,0:T(2,128)S(1)} all-gather(f32[1,2,2048]{2,1,0:T(2,128)S(1)} %convolution_bitcast_fusion), channel_id=8, replica_groups=mesh['sp_0'=8,'sp_1'=4,'tp'=4,'dp'=2] {'sp_0'}, dimensions={0}, use_global_device_ids=true | all-gather | bytes 147456 | tf_op jit(solution)/shard_map/all_gather | solution.py:19
  36.8 12.3 %all-gather.13 = f32[4,2,2048]{2,1,0:T(2,128)S(1)} all-gather(f32[1,2,2048]{2,1,0:T(2,128)S(1)} %bitcast.343), channel_id=9, replica_groups=mesh['sp_0'=8,'sp_1'=4,'tp'=4,'dp'=2] {'sp_1'}, dimensions={0}, use_global_device_ids=true | all-gather | bytes 81920 | tf_op jit(solution)/shard_map/all_gather | solution.py:19
  49.1 12.1 %all-gather.14 = f32[4,2,2048]{2,1,0:T(2,128)S(1)} all-gather(f32[1,2,2048]{2,1,0:T(2,128)S(1)} %bitcast.344), channel_id=10, replica_groups=mesh['sp_0'=8,'sp_1'=4,'tp'=4,'dp'=2] {'tp'}, dimensions={0}, use_global_device_ids=true | all-gather | bytes 81920 | tf_op jit(solution)/shard_map/all_gather | solution.py:19
  62.2 24.6 %all-gather.9 = f32[8,2,2048]{2,1,0:T(2,128)S(1)} all-gather(f32[1,2,2048]{2,1,0:T(2,128)S(1)} %convolution_bitcast_fusion.1), channel_id=5, replica_groups=mesh['sp_0'=8,'sp_1'=4,'tp'=4,'dp'=2] {'sp_0'}, dimensions={0}, use_global_device_ids=true | all-gather | bytes 147456 | tf_op jit(solution)/shard_map/all_gather | solution.py:19
  86.8 11.9 %all-gather.10 = f32[4,2,2048]{2,1,0:T(2,128)S(1)} all-gather(f32[1,2,2048]{2,1,0:T(2,128)S(1)} %bitcast.345), channel_id=6, replica_groups=mesh['sp_0'=8,'sp_1'=4,'tp'=4,'dp'=2] {'sp_1'}, dimensions={0}, use_global_device_ids=true | all-gather | bytes 81920 | tf_op jit(solution)/shard_map/all_gather | solution.py:19
  98.7 11.9 %all-gather.11 = f32[4,2,2048]{2,1,0:T(2,128)S(1)} all-gather(f32[1,2,2048]{2,1,0:T(2,128)S(1)} %bitcast.346), channel_id=7, replica_groups=mesh['sp_0'=8,'sp_1'=4,'tp'=4,'dp'=2] {'tp'}, dimensions={0}, use_global_device_ids=true | all-gather | bytes 81920 | tf_op jit(solution)/shard_map/all_gather | solution.py:19
  123.4 20.7 %all-gather.19.cloned.1.call-done = bf16[512,2048]{1,0:T(8,128)(2,1)} async-done(((bf16[128,2048]{1,0:T(8,128)(2,1)}), bf16[512,2048]{1,0:T(8,128)(2,1)}) %all-gather.19.cloned.1.call-update) | async-done | bytes 2097168 | tf_op jit(solution)/shard_map/all_gather | solution.py:167
  144.1 3.5 convolution_convert_fusion.2
  149.3 8.3 %rev.32 = bf16[512,512]{1,0:T(8,128)(2,1)} reverse(bf16[512,512]{1,0:T(8,128)(2,1)} %bitcast.317), dimensions={0} | reverse | bytes 1048576 | tf_op jit(solution)/shard_map/rev | solution.py:206
  157.6 2.9 reshape.600
  185.0 3.7 fusion.75
  190.2 8.1 %while.27 = (s32[]{:T(128)}, f32[2,4,128,64]{3,2,1,0:T(8,128)S(1)}, f32[4,2,4,128,64]{4,3,2,1,0:T(8,128)}, f32[4,2,4]{2,1,0:T(2,128)S(1)}, f32[4,2,4,128,64]{4,3,2,1,0:T(8,128)}, /*index=5*/s32[]{:T(128)}, s32[]{:T(128)}) while((s32[]{:T(128)}, f32[2,4,128,64]{3,2,1,0:T(8,128)S(1)}, f32[4,2,4,128,64]{4,3,2,1,0:T(8,128)}, ...), condition=%wide.region_19.20_spmd.clone, body=%wide.region_18.19_spmd.clone.sunk | while | flops 262147 | bytes 1573068 | solution.py:96
  203.7 3.0 reshape.599
  217.3 10.8 %while.26 = (s32[]{:T(128)}, f32[2,4,128,64]{3,2,1,0:T(8,128)S(1)}, f32[4,2,4,128,64]{4,3,2,1,0:T(8,128)}, f32[4,2,4]{2,1,0:T(2,128)}, f32[4,2,4,128,64]{4,3,2,1,0:T(8,128)}, /*index=5*/s32[]{:T(128)}, s32[]{:T(128)}) while((s32[]{:T(128)}, f32[2,4,128,64]{3,2,1,0:T(8,128)S(1)}, f32[4,2,4,128,64]{4,3,2,1,0:T(8,128)}, ...), condition=%wide.region_13.14_spmd.clone, body=%wide.region_12.13_spmd.clone.sunk | while | flops 262147 | bytes 1573068 | solution.py:96
  254.4 3.8 multiply_convert_fusion.5
  266.0 3.0 rev.33
  273.1 52.2 %all_gather.85 = bf16[16384,16]{0,1:T(8,128)(2,1)S(1)} all-gather(bf16[512,16]{0,1:T(8,128)(2,1)S(1)} %convolution_convert_fusion.7), channel_id=1, replica_groups=mesh['sp_0'=8,'sp_1'=4,'tp'=4,'dp'=2] {'sp_0','sp_1'}, dimensions={0}, use_global_device_ids=true | all-gather | bytes 540672 | tf_op jit(solution)/shard_map/all_gather | solution.py:220
  337.0 3.0 convolution_bitcast_fusion.3
  341.9 4.5 %multiply_reduce_fusion.1 = (f32[8,128,64]{1,2,0:T(8,128)S(1)}, f32[8,128,64]{1,2,0:T(8,128)S(1)}) fusion(bf16[32,16,128,64]{2,3,1,0:T(8,128)(2,1)} %all-gather.21.cloned.1.call-done, f32[32,8]{1,0:T(8,128)S(1)} %exponential_select_fusion.1, f32[32,8]{1,0:T(8,128)S(1)} %get-tuple-element.212), kind=kLoop, calls=%fused_computation.7 | loop fusion | flops 12451840 | bytes 8914944 | tf_op jit(solution)/shard_map/reduce_sum | solution.py:275
  353.3 5.9 %rev.37 = f32[512,512]{0,1:T(8,128)} reverse(f32[512,512]{0,1:T(8,128)S(1)} %bitcast.319), dimensions={0} | reverse | bytes 2097152 | tf_op jit(solution)/shard_map/rev | solution.py:296
  371.0 6.0 %all-to-all-start = ((bf16[4,128,2048]{2,1,0:T(8,128)(2,1)}), bf16[4,128,2048]{2,1,0:T(8,128)(2,1)}, u32[]{:S(2)}, u32[]{:S(2)}) async-start(bf16[4,128,2048]{2,1,0:T(8,128)(2,1)} %bitcast.323), calls=%async_computation | async-start | bytes 4194304 | tf_op jit(solution)/shard_map/all_to_all | solution.py:38
  377.2 24.7 %all-gather = f32[16384]{0:T(1024)S(1)} all-gather(f32[2048]{0:T(1024)S(1)} %bitcast.353), channel_id=2, replica_groups=mesh['sp_0'=8,'sp_1'=4,'tp'=4,'dp'=2] {'sp_0'}, dimensions={0}, use_global_device_ids=true | all-gather | bytes 73728 | tf_op jit(solution)/shard_map/all_gather | solution.py:19
  402.0 11.9 %all-gather.1 = f32[8192]{0:T(1024)S(1)} all-gather(f32[2048]{0:T(1024)S(1)} %reduce.6), channel_id=3, replica_groups=mesh['sp_0'=8,'sp_1'=4,'tp'=4,'dp'=2] {'sp_1'}, dimensions={0}, use_global_device_ids=true | all-gather | bytes 40960 | tf_op jit(solution)/shard_map/all_gather | solution.py:19
  413.9 11.9 %all-gather.2 = f32[8192]{0:T(1024)S(1)} all-gather(f32[2048]{0:T(1024)S(1)} %reduce.7), channel_id=4, replica_groups=mesh['sp_0'=8,'sp_1'=4,'tp'=4,'dp'=2] {'tp'}, dimensions={0}, use_global_device_ids=true | all-gather | bytes 40960 | tf_op jit(solution)/shard_map/all_gather | solution.py:19
  (312 shorter events, 150.9 us)
Async XLA Ops:
  6.5 361.9 %copy-start = (bf16[512,2048]{1,0:T(8,128)(2,1)S(1)}, bf16[512,2048]{1,0:T(8,128)(2,1)}, u32[]{:S(2)}) copy-start(bf16[512,2048]{1,0:T(8,128)(2,1)} %param.41) | copy-start | bytes 6291460
  6.5 105.3 %copy-start.1 = (bf16[1,128,2048]{2,1,0:T(8,128)(2,1)S(1)}, bf16[1,128,2048]{2,1,0:T(8,128)(2,1)}, u32[]{:S(2)}) copy-start(bf16[1,128,2048]{2,1,0:T(8,128)(2,1)} %param.23) | copy-start | bytes 1572868
  6.5 137.6 %all-gather.19.cloned.1.call-start = ((), (), s32[]{:S(2)}) async-start(), calls=%async_computation.1 | async-start | bytes 2621440 | tf_op jit(solution)/shard_map/all_gather | solution.py:167
  6.5 107.0 %copy-start.16 = (bf16[1,32,2048]{2,1,0:T(8,128)(2,1)S(1)}, bf16[1,32,2048]{2,1,0:T(8,128)(2,1)}, u32[]{:S(2)}) copy-start(bf16[1,32,2048]{2,1,0:T(8,128)(2,1)} %param.25) | copy-start | bytes 393220
  7.5 54.7 %copy-start.48 = (bf16[2,16]{1,0:T(2,128)(2,1)}, bf16[2,16]{1,0:T(2,128)(2,1)S(1)}, u32[]{:S(2)}) copy-start(bf16[2,16]{1,0:T(2,128)(2,1)S(1)} %fusion.152) | copy-start | bytes 196
  36.7 77.2 %copy-start.40 = (bf16[2048,2,32]{0,2,1:T(8,128)(2,1)S(1)}, bf16[2048,2,32]{0,2,1:T(8,128)(2,1)}, u32[]{:S(2)}) copy-start(bf16[2048,2,32]{0,2,1:T(8,128)(2,1)} %param.34) | copy-start | bytes 786436
  113.4 120.0 %all-gather.23.cloned.1.call-start = ((), (), s32[]{:S(2)}) async-start(), calls=%async_computation.3 | async-start | bytes 1892352 | tf_op jit(solution)/shard_map/all_gather | solution.py:26
  118.5 223.4 %all-gather.21.cloned.1.call-start = ((), (), s32[]{:S(2)}) async-start(), calls=%async_computation.2 | async-start | bytes 8650752 | tf_op jit(solution)/shard_map/all_gather | solution.py:26
  119.8 45.3 %copy-start.50 = (f32[8]{0:T(128)}, f32[8]{0:T(128)S(1)}, u32[]{:S(2)}) copy-start(f32[8]{0:T(128)S(1)} %get-tuple-element.233) | copy-start | bytes 100
  121.6 26.1 %copy-start.30 = (f32[1,512]{1,0:T(1,128)}, f32[1,512]{1,0:T(1,128)S(1)}, u32[]{:S(2)}) copy-start(f32[1,512]{1,0:T(1,128)S(1)} %get-tuple-element.205) | copy-start | bytes 6148
  121.6 26.1 %copy-start.32 = (f32[1,512]{1,0:T(1,128)}, f32[1,512]{1,0:T(1,128)S(1)}, u32[]{:S(2)}) copy-start(f32[1,512]{1,0:T(1,128)S(1)} %get-tuple-element.206) | copy-start | bytes 6148
  121.6 26.1 %copy-start.34 = (f32[1,512]{1,0:T(1,128)}, f32[1,512]{1,0:T(1,128)S(1)}, u32[]{:S(2)}) copy-start(f32[1,512]{1,0:T(1,128)S(1)} %get-tuple-element.207) | copy-start | bytes 6148
  121.6 26.1 %copy-start.36 = (f32[1,512]{1,0:T(1,128)}, f32[1,512]{1,0:T(1,128)S(1)}, u32[]{:S(2)}) copy-start(f32[1,512]{1,0:T(1,128)S(1)} %get-tuple-element.208) | copy-start | bytes 6148
  123.4 53.3 %copy-start.43 = (f32[1,256]{1,0:T(1,128)}, f32[1,256]{1,0:T(1,128)S(1)}, u32[]{:S(2)}) copy-start(f32[1,256]{1,0:T(1,128)S(1)} %get-tuple-element.216) | copy-start | bytes 3076
  123.4 53.3 %copy-start.44 = (f32[1,256]{1,0:T(1,128)}, f32[1,256]{1,0:T(1,128)S(1)}, u32[]{:S(2)}) copy-start(f32[1,256]{1,0:T(1,128)S(1)} %get-tuple-element.217) | copy-start | bytes 3076
  123.4 53.3 %copy-start.45 = (f32[1,256]{1,0:T(1,128)}, f32[1,256]{1,0:T(1,128)S(1)}, u32[]{:S(2)}) copy-start(f32[1,256]{1,0:T(1,128)S(1)} %get-tuple-element.218) | copy-start | bytes 3076
  123.4 53.3 %copy-start.46 = (f32[1,256]{1,0:T(1,128)}, f32[1,256]{1,0:T(1,128)S(1)}, u32[]{:S(2)}) copy-start(f32[1,256]{1,0:T(1,128)S(1)} %get-tuple-element.219) | copy-start | bytes 3076
  123.4 53.3 %copy-start.47 = (f32[1,256]{1,0:T(1,128)}, f32[1,256]{1,0:T(1,128)S(1)}, u32[]{:S(2)}) copy-start(f32[1,256]{1,0:T(1,128)S(1)} %get-tuple-element.220) | copy-start | bytes 3076
  270.0 59.3 %copy-start.11 = (bf16[8,64,256]{2,1,0:T(8,128)(2,1)S(1)}, bf16[8,64,256]{2,1,0:T(8,128)(2,1)}, u32[]{:S(2)}) copy-start(bf16[8,64,256]{2,1,0:T(8,128)(2,1)} %copy-done.10) | copy-start | bytes 786436
  273.1 63.8 %copy-start.15 = (bf16[4,128,2,4,64]{1,4,3,2,0:T(8,128)(2,1)S(1)}, bf16[4,128,2,4,64]{1,4,3,2,0:T(8,128)(2,1)}, u32[]{:S(2)}) copy-start(bf16[4,128,2,4,64]{1,4,3,2,0:T(8,128)(2,1)} %copy-done.14) | copy-start | bytes 1572868
  273.1 63.8 %copy-start.25 = (f32[4,128,2,4]{1,3,2,0:T(4,128)S(1)}, f32[4,128,2,4]{1,3,2,0:T(4,128)}, u32[]{:S(2)}) copy-start(f32[4,128,2,4]{1,3,2,0:T(4,128)} %get-tuple-element.196) | copy-start | bytes 49156
  273.1 63.8 %copy-start.26 = (f32[4,128,2,4]{1,3,2,0:T(4,128)S(1)}, f32[4,128,2,4]{1,3,2,0:T(4,128)}, u32[]{:S(2)}) copy-start(f32[4,128,2,4]{1,3,2,0:T(4,128)} %copy.282) | copy-start | bytes 49156
  371.0 54.9 %all-to-all-start = ((bf16[4,128,2048]{2,1,0:T(8,128)(2,1)}), bf16[4,128,2048]{2,1,0:T(8,128)(2,1)}, u32[]{:S(2)}, u32[]{:S(2)}) async-start(bf16[4,128,2048]{2,1,0:T(8,128)(2,1)} %bitcast.323), calls=%async_computation | async-start | bytes 4194304 | tf_op jit(solution)/shard_map/all_to_all | solution.py:38
  377.1 50.9 %copy-start.2 = (bf16[1,128,2048]{2,1,0:T(8,128)(2,1)S(1)}, bf16[1,128,2048]{2,1,0:T(8,128)(2,1)}, u32[]{:S(2)}) copy-start(bf16[1,128,2048]{2,1,0:T(8,128)(2,1)} %param.23) | copy-start | bytes 1572868
  (44 other events, 197.6 us)
Sparse Core Ops, SparseCore 0:
  113.6 30.5 all-gather.18
  146.7 78.5 all-gather.22
  229.1 101.3 all-gather.20
